TPU v7x, 32 devices: a whole 2x2x4 slice. The times are simulated.
32 devices in a mesh: sp: 8 (over z, x), tp: 4 (over y, core).
Axes of the slice: x: 2, y: 2, z: 4, core: 2. Of those that a mesh axis runs over, the one named last changes fastest.
Arguments:
- residual: bfloat16 [2048, 2048], P(('sp', 'tp')), may hold values from -6 to 6
- queries: bfloat16 [2048, 512], P('sp', 'tp'), may hold values from -6 to 6
- projected_keys: bfloat16 [2048, 512], P('sp', 'tp'), may hold values from -6 to 6
- values: bfloat16 [2048, 1024], P('sp', 'tp'), may hold values from -6 to 6
- projected_output_gate: bfloat16 [2048, 1024], P('sp', 'tp'), may hold values from -6 to 6
- decay_gate_input: bfloat16 [2048, 512], P('sp', 'tp'), may hold values from -7 to 7
- decay_gate_offset: float32 [512], P('tp')
- decay_spikes: float32 [2048, 16], P('sp', 'tp'), may hold values from -3 to 0, as said below
- documents: int32 [2048], P('sp'), may hold values from 0 to 3, as said below
- attention_output_weight: bfloat16 [1024, 2048], P('tp'), may hold values from -0.1875 to 0.1875
- layer_norm_gains: float32 [2, 2048], replicated, may hold values from 0.1 to 1.9
- layer_norm_shifts: float32 [2, 2048], replicated, may hold values from -3 to 3
- routes: int32 [2048, 2], P('sp'), may hold values from 0 to 7, all different within a row; in each aligned block of 64 rows (0 to 63, 64 to 127, ...) at most 32 rows name the same one
- chosen_expert_weights: float32 [2048, 2], P('sp'), may hold values from 0.2 to 1
- expert_gate_weight: bfloat16 [8, 2048, 3584], P('sp', None, 'tp'), may hold values from -0.125 to 0.125
- expert_up_weight: bfloat16 [8, 2048, 3584], P('sp', None, 'tp'), may hold values from -0.125 to 0.125
- expert_down_weight: bfloat16 [8, 3584, 2048], P('sp', 'tp'), may hold values from -0.09375 to 0.09375
Outputs:
- layer_out: bfloat16 [2048, 2048], P(('sp', 'tp'))
Inputs may be any that keep to these rules, and one draw needn't show every extreme that they name: `routes`: each row names 2 different experts; in each aligned block of 64 rows no expert is named by more than 32 rows. `documents`: the first position has document 0; document numbers never fall and rise by at most one from a position to the next. `decay_spikes`: zero at all but a few positions.
All inputs are finite; a program needn't handle non-finite values.
Results may differ from a plain program's by a relative error of at most 0.015.
Values may be sent and summed in bfloat16 or wider, within the bound.
A program may use at most 64 MiB of HBM per device.

v0:
```python
import functools
import jax
import jax.numpy as jnp
from jax import lax
from jax.experimental import pallas as pl
from jax.experimental.pallas import tpu as pltpu
from jax.sharding import PartitionSpec as P

MESH = pl.DeviceIdType.MESH
VMEM = pl.BlockSpec(memory_space=pltpu.VMEM)
NT = (((1,), (1,)), ((), ()))
TN = (((0,), (0,)), ((), ()))


def silu(v):
    return v / (1.0 + jnp.exp(-v))


def halfway_totals(totals, half):
    rows, width = totals.shape
    if half >= 4:
        grouped = totals.reshape(rows // (2 * half), 2 * half, width)
        return jnp.broadcast_to(grouped[:, half - 1 : half, :], grouped.shape).reshape(rows, width)
    row = lax.broadcasted_iota(jnp.int32, totals.shape, 0) % (2 * half)
    found = totals
    for place in range(2 * half):
        shift = place - (half - 1)
        if shift:
            found = jnp.where(row == place, pltpu.roll(totals, shift % rows, 0), found)
    return found


def attention_kernel(
    heads, sp_count, tp_count,
    q_ref, k_ref, v_ref, gate_ref, decay_ref, offset_ref, spikes_ref, doc_col_ref, doc_row_ref,
    weight_ref, residual_ref, gains_ref, shifts_ref,
    normed_ref,
    state_out, state_in, state_acc, decay_acc, doc_acc, mixed_ref,
    part_send, part_in, pair_send, pair_in,
    state_send_sem, state_recv_sem, part_send_sem, part_recv_sem, pair_sems,
):
    here = lax.axis_index("sp")
    me = lax.axis_index("tp")
    core = me % 2
    side = me // 2
    partner = side * 2 + (1 - core)
    across = (1 - side) * 2 + core
    rows = q_ref.shape[0]
    key_dim = q_ref.shape[1] // heads
    value_dim = v_ref.shape[1] // heads
    own_rows = residual_ref.shape[0]

    barrier = pltpu.get_barrier_semaphore()

    def greet(k, carry):
        @pl.when(k != here)
        def _():
            pl.semaphore_signal(barrier, inc=1, device_id={"sp": k}, device_id_type=MESH)
        return carry

    lax.fori_loop(0, sp_count, greet, 0)
    pl.semaphore_signal(barrier, inc=1, device_id={"tp": partner}, device_id_type=MESH)
    pl.semaphore_signal(barrier, inc=1, device_id={"tp": across}, device_id_type=MESH)

    x = decay_ref[...].astype(jnp.float32) + offset_ref[...]
    rate = (jnp.minimum(x, 0.0) - jnp.log1p(jnp.exp(-jnp.abs(x)))) * (1.0 / 16.0)
    lane_head = lax.broadcasted_iota(jnp.int32, rate.shape, 1) // key_dim
    spikes = spikes_ref[...]
    extra = jnp.zeros_like(rate)
    for h in range(heads):
        extra = jnp.where(lane_head == h, spikes[:, h : h + 1], extra)
    totals = rate + extra
    row_of = lax.broadcasted_iota(jnp.int32, rate.shape, 0)
    step = 1
    while step < rows:
        totals = totals + jnp.where(row_of >= step, pltpu.roll(totals, step, 0), 0.0)
        step *= 2
    doc_col = doc_col_ref[...]
    doc_row = doc_row_ref[...]
    last_total = totals[rows - 1 : rows, :]
    last_doc = doc_row[:, rows - 1 : rows]
    key = k_ref[...].astype(jnp.float32)
    query = q_ref[...].astype(jnp.float32) * key_dim ** (-0.5)
    ends = (key * jnp.exp(last_total - totals) * (doc_col == last_doc).astype(jnp.float32)).astype(
        jnp.bfloat16
    )
    values = v_ref[...]
    state = jnp.concatenate(
        [
            lax.dot_general(
                values[:, h * value_dim : (h + 1) * value_dim],
                ends[:, h * key_dim : (h + 1) * key_dim],
                TN,
                preferred_element_type=jnp.float32,
            )
            for h in range(heads)
        ],
        axis=1,
    )
    state_out[0:value_dim, :] = state.astype(jnp.bfloat16)
    tail_shape = (state_out.shape[0] - value_dim, rate.shape[1])
    tail_row = lax.broadcasted_iota(jnp.int32, tail_shape, 0)
    state_out[value_dim:, :] = jnp.where(
        tail_row == 0, jnp.exp(last_total), last_doc.astype(jnp.float32)
    ).astype(jnp.bfloat16)
    pl.semaphore_wait(barrier, sp_count + 1)

    def state_copy(target, slot):
        return pltpu.make_async_remote_copy(
            src_ref=state_out,
            dst_ref=state_in.at[slot],
            send_sem=state_send_sem.at[target],
            recv_sem=state_recv_sem.at[slot],
            device_id={"sp": target},
            device_id_type=MESH,
        )

    def send_state(j, carry):
        target = sp_count - 1 - j

        @pl.when(target > here)
        def _():
            state_copy(target, here).start()
        return carry

    lax.fori_loop(0, sp_count, send_state, 0)

    t_of = lax.broadcasted_iota(jnp.int32, (rows, rows), 0)
    s_of = lax.broadcasted_iota(jnp.int32, (rows, rows), 1)
    apart = t_of ^ s_of
    visible = (t_of >= s_of) & (doc_col == doc_row)
    halves = []
    half = 1
    while half < rows:
        halves.append(half)
        half *= 2
    scaled = [(0, query.astype(jnp.bfloat16), k_ref[...])]
    for half in halves:
        fade = jnp.exp(-jnp.abs(totals - halfway_totals(totals, half)))
        scaled.append((half, (query * fade).astype(jnp.bfloat16), (key * fade).astype(jnp.bfloat16)))
    inner = []
    for h in range(heads):
        span = slice(h * key_dim, (h + 1) * key_dim)
        scores = None
        for half, q_part, k_part in scaled:
            product = lax.dot_general(
                q_part[:, span], k_part[:, span], NT, preferred_element_type=jnp.float32
            )
            scores = product if scores is None else jnp.where(apart >= half, product, scores)
        scores = jnp.where(visible, scores, 0.0).astype(jnp.bfloat16)
        inner.append(
            jnp.dot(
                scores,
                values[:, h * value_dim : (h + 1) * value_dim],
                preferred_element_type=jnp.float32,
            )
        )

    state_acc[...] = jnp.zeros_like(state_acc)
    decay_acc[...] = jnp.ones_like(decay_acc)
    doc_acc[...] = jnp.full_like(doc_acc, -1.0)

    def join(j, carry):
        k = here - 1 - j

        @pl.when(k >= 0)
        def _():
            state_copy(here, k).wait_recv()
            tail = state_in[k, value_dim:, :].astype(jnp.float32)
            doc_k = tail[1:2, :]

            @pl.when(j == 0)
            def _():
                doc_acc[...] = doc_k

            factor = jnp.where(doc_k == doc_acc[...], decay_acc[...], 0.0)
            state_acc[...] += state_in[k, 0:value_dim, :].astype(jnp.float32) * factor
            decay_acc[...] = factor * tail[0:1, :]
        return carry

    lax.fori_loop(0, sp_count, join, 0)
    prefix = state_acc[...].astype(jnp.bfloat16)
    active = (doc_col.astype(jnp.float32) == doc_acc[...]).astype(jnp.float32)
    entering = (query * jnp.exp(totals) * active).astype(jnp.bfloat16)
    for h in range(heads):
        span = slice(h * key_dim, (h + 1) * key_dim)
        out_span = slice(h * value_dim, (h + 1) * value_dim)
        recurrent = inner[h] + lax.dot_general(
            entering[:, span], prefix[:, span], NT, preferred_element_type=jnp.float32
        )
        scale = lax.rsqrt(jnp.mean(recurrent * recurrent, axis=-1, keepdims=True) + 1e-6)
        gate = silu(gate_ref[:, out_span].astype(jnp.float32))
        mixed_ref[:, out_span] = (recurrent * scale * gate).astype(jnp.bfloat16)

    def share(index):
        begin = pl.multiple_of(index * own_rows, own_rows)
        return jnp.dot(
            mixed_ref[pl.ds(begin, own_rows), :], weight_ref[...], preferred_element_type=jnp.float32
        )

    def part_copy(slot):
        return pltpu.make_async_remote_copy(
            src_ref=part_send.at[slot],
            dst_ref=part_in.at[slot],
            send_sem=part_send_sem.at[slot],
            recv_sem=part_recv_sem.at[slot],
            device_id={"tp": partner},
            device_id_type=MESH,
        )

    pair_copy = pltpu.make_async_remote_copy(
        src_ref=pair_send,
        dst_ref=pair_in,
        send_sem=pair_sems.at[0],
        recv_sem=pair_sems.at[1],
        device_id={"tp": across},
        device_id_type=MESH,
    )
    part_send[0] = share((1 - side) * 2 + (1 - core)).astype(jnp.bfloat16)
    part_copy(0).start()
    part_send[1] = share(side * 2 + (1 - core)).astype(jnp.bfloat16)
    part_copy(1).start()
    far = share(across)
    part_copy(0).wait_recv()
    pair_send[...] = (far + part_in[0].astype(jnp.float32)).astype(jnp.bfloat16)
    pair_copy.start()
    near = share(me) + residual_ref[...].astype(jnp.float32)
    part_copy(1).wait_recv()
    near = near + part_in[1].astype(jnp.float32)
    pair_copy.wait_recv()
    near = near + pair_in[...].astype(jnp.float32)
    normed_ref[...] = norm_rows(near, gains_ref[0:1, :], shifts_ref[0:1, :]).astype(jnp.bfloat16)
    part_copy(0).wait_send()
    part_copy(1).wait_send()
    pair_copy.wait_send()

    def finish(j, carry):
        @pl.when(j > here)
        def _():
            state_copy(j, here).wait_send()
        return carry

    lax.fori_loop(0, sp_count, finish, 0)


def norm_rows(stream, gain, shift):
    center = jnp.mean(stream, axis=-1, keepdims=True)
    moved = stream - center
    spread = jnp.mean(moved * moved, axis=-1, keepdims=True)
    return moved * lax.rsqrt(spread + 1e-5) * gain + shift


def attention(sp_count, tp_count, residual, q, k, v, gate, decay_in, offset, spikes, documents, weight, gains, shifts):
    rows, heads = spikes.shape
    own_rows, width = residual.shape
    channels = q.shape[1]
    value_dim = v.shape[1] // heads
    state_rows = value_dim + 16
    return pl.pallas_call(
        functools.partial(attention_kernel, heads, sp_count, tp_count),
        out_shape=jax.ShapeDtypeStruct((own_rows, width), jnp.bfloat16),
        in_specs=[VMEM] * 13,
        out_specs=VMEM,
        scratch_shapes=[
            pltpu.VMEM((state_rows, channels), jnp.bfloat16),
            pltpu.VMEM((sp_count, state_rows, channels), jnp.bfloat16),
            pltpu.VMEM((value_dim, channels), jnp.float32),
            pltpu.VMEM((1, channels), jnp.float32),
            pltpu.VMEM((1, channels), jnp.float32),
            pltpu.VMEM((rows, v.shape[1]), jnp.bfloat16),
            pltpu.VMEM((2, own_rows, width), jnp.bfloat16),
            pltpu.VMEM((2, own_rows, width), jnp.bfloat16),
            pltpu.VMEM((own_rows, width), jnp.bfloat16),
            pltpu.VMEM((own_rows, width), jnp.bfloat16),
            pltpu.SemaphoreType.DMA((sp_count,)),
            pltpu.SemaphoreType.DMA((sp_count,)),
            pltpu.SemaphoreType.DMA((2,)),
            pltpu.SemaphoreType.DMA((2,)),
            pltpu.SemaphoreType.DMA((2,)),
        ],
        compiler_params=pltpu.CompilerParams(
            collective_id=0, has_side_effects=True, vmem_limit_bytes=48 * 1024 * 1024
        ),
        name="attention",
    )(
        q, k, v, gate, decay_in, offset.reshape(1, -1), spikes, documents.reshape(-1, 1),
        documents.reshape(1, -1), weight, residual, gains, shifts,
    )

def flipped(index, mask):
    bit, result = 1, index
    while bit <= mask:
        if mask & bit:
            result = result + bit * (1 - 2 * ((index // bit) % 2))
        bit *= 2
    return result


def experts_kernel(
    sp_count, tp_count, cap,
    normed_ref, routes_ref, chosen_ref, gains_ref, shifts_ref, gate_hbm, up_hbm, down_hbm,
    out_ref,
    outgoing, rows, partial, gate_up, down, hidden, pair_in, far_out, far_in, final, returned,
    weight_sems, a_send, a_recv, y_send, y_recv, p_send, p_recv,
    r_send, r_recv, f_send, f_recv, b_send, b_recv,
):
    here = lax.axis_index("sp")
    me = lax.axis_index("tp")
    core = me % 2
    side = me // 2
    partner = side * 2 + (1 - core)
    across = (1 - side) * 2 + core
    diagonal = (1 - side) * 2 + (1 - core)
    tokens, width = normed_ref.shape
    slot_total = sp_count * cap
    tile = 128
    tiles = gate_hbm.shape[2] // tile
    group = 2 * tp_count * cap
    pairs = sp_count // 2

    barrier = pltpu.get_barrier_semaphore()

    def greet(k, carry):
        @pl.when(k != here)
        def _():
            pl.semaphore_signal(barrier, inc=1, device_id={"sp": k}, device_id_type=MESH)
        return carry

    lax.fori_loop(0, sp_count, greet, 0)
    pl.semaphore_signal(barrier, inc=1, device_id={"tp": partner}, device_id_type=MESH)
    pl.semaphore_signal(barrier, inc=1, device_id={"tp": across}, device_id_type=MESH)

    weight_copies = []
    for j in range(tiles):
        for kind, source in enumerate((gate_hbm, up_hbm)):
            weight_copies.append(
                pltpu.make_async_copy(
                    source.at[0, :, pl.ds(j * tile, tile)],
                    gate_up.at[j, :, pl.ds(kind * tile, tile)],
                    weight_sems.at[2 * j + kind],
                )
            )
    weight_copies.append(pltpu.make_async_copy(down_hbm.at[0], down, weight_sems.at[2 * tiles]))
    for copy in weight_copies:
        copy.start()

    begin = pl.multiple_of(me * tokens, tokens)
    routes = routes_ref[pl.ds(begin, tokens), :]
    chosen = chosen_ref[pl.ds(begin, tokens), :]
    expert_lane = lax.broadcasted_iota(jnp.int32, (tokens, 128), 1)
    marks = [(routes[:, j : j + 1] == expert_lane).astype(jnp.float32) for j in range(2)]
    earlier = (
        lax.broadcasted_iota(jnp.int32, (tokens, tokens), 0)
        > lax.broadcasted_iota(jnp.int32, (tokens, tokens), 1)
    ).astype(jnp.float32)
    before = jnp.dot(
        earlier.astype(jnp.bfloat16),
        (marks[0] + marks[1]).astype(jnp.bfloat16),
        preferred_element_type=jnp.float32,
    )
    slot_lane = lax.broadcasted_iota(jnp.int32, (tokens, slot_total), 1).astype(jnp.float32)
    picks = []
    for j in range(2):
        position = jnp.sum(before * marks[j], axis=1, keepdims=True)
        slot = routes[:, j : j + 1].astype(jnp.float32) * float(cap) + position
        picks.append((slot_lane == slot).astype(jnp.bfloat16))
    outgoing[...] = lax.dot_general(
        picks[0] + picks[1], normed_ref[...], TN, preferred_element_type=jnp.float32
    ).astype(jnp.bfloat16)

    def block(ref, index):
        return ref.at[pl.ds(pl.multiple_of(index * cap, cap), cap), :]

    def load(ref, index):
        return ref[pl.ds(pl.multiple_of(index * cap, cap), cap), :]

    def remote(src, dst, send_sem, recv_sem, target):
        return pltpu.make_async_remote_copy(
            src_ref=src, dst_ref=dst, send_sem=send_sem, recv_sem=recv_sem,
            device_id=target, device_id_type=MESH,
        )

    def row_block(source, part):
        return block(rows, source * tp_count + part)

    def dispatch(target, source):
        return remote(
            block(outgoing, target), row_block(source, me), a_send.at[target], a_recv.at[source],
            {"sp": target},
        )

    def to_across(source, part):
        return remote(
            row_block(source, part), row_block(source, part), y_send.at[source], y_recv.at[source],
            {"tp": across},
        )

    def to_partner(source, turn, part):
        return remote(
            row_block(source, part), row_block(source, part),
            p_send.at[source, turn], p_recv.at[source, turn], {"tp": partner},
        )

    def part_to_partner(source, turn):
        part = partner if turn == 0 else diagonal
        return remote(
            block(partial, source * tp_count + part), block(pair_in, source * 2 + turn),
            r_send.at[source, turn], r_recv.at[source, turn], {"tp": partner},
        )

    def pair_to_across(source):
        return remote(
            block(far_out, source), block(far_in, source), f_send.at[source], f_recv.at[source],
            {"tp": across},
        )

    def give_back(source, expert):
        return remote(
            block(final, source), block(returned, expert), b_send.at[source], b_recv.at[expert],
            {"sp": source},
        )

    pl.semaphore_wait(barrier, sp_count + 1)
    for k in range(1, sp_count):
        dispatch(flipped(here, k), here).start()
    own = pl.multiple_of((here * tp_count + me) * cap, cap)
    rows[pl.ds(own, cap), :] = load(outgoing, here)

    def sources_of(p):
        base = flipped(here // 2, p) * 2
        return (base + here % 2, base + 1 - here % 2)

    def spread(p):
        for n, source in enumerate(sources_of(p)):
            if p or n:
                dispatch(source, source).wait_recv()
            to_across(source, me).start()
            to_partner(source, 0, me).start()

    def relay(p):
        for source in sources_of(p):
            to_across(source, across).wait_recv()
            to_partner(source, 1, across).start()

    def compute(p):
        for source in sources_of(p):
            to_partner(source, 0, partner).wait_recv()
            to_partner(source, 1, diagonal).wait_recv()
        base = pl.multiple_of(flipped(here // 2, p) * group, group)

        def first(j, carry):
            both = jnp.dot(
                rows[pl.ds(base, group), :], gate_up[j], preferred_element_type=jnp.float32
            )
            unit = (silu(both[:, :tile]) * both[:, tile:]).astype(jnp.bfloat16)
            hidden[:, pl.ds(pl.multiple_of(j * tile, tile), tile)] = unit
            return carry

        lax.fori_loop(0, tiles, first, 0)
        span = 512

        def second(j, carry):
            lanes = pl.ds(pl.multiple_of(j * span, span), span)
            partial[pl.ds(base, group), lanes] = jnp.dot(
                hidden[...], down[:, lanes], preferred_element_type=jnp.float32
            ).astype(jnp.bfloat16)
            return carry

        lax.fori_loop(0, width // span, second, 0)
        for turn in (1, 0):
            for source in sources_of(p):
                part_to_partner(source, turn).start()

    def fold(p):
        for source in sources_of(p):
            part_to_partner(source, 1).wait_recv()
            far_out[pl.ds(pl.multiple_of(source * cap, cap), cap), :] = (
                load(partial, source * tp_count + across).astype(jnp.float32)
                + load(pair_in, source * 2 + 1).astype(jnp.float32)
            ).astype(jnp.bfloat16)
            pair_to_across(source).start()

    def finish(p):
        for n, source in enumerate(sources_of(p)):
            part_to_partner(source, 0).wait_recv()
            pair_to_across(source).wait_recv()
            value = (
                load(partial, source * tp_count + me).astype(jnp.float32)
                + load(pair_in, source * 2).astype(jnp.float32)
                + load(far_in, source).astype(jnp.float32)
            ).astype(jnp.bfloat16)
            if p or n:
                final[pl.ds(pl.multiple_of(source * cap, cap), cap), :] = value
                give_back(source, here).start()
            else:
                returned[pl.ds(pl.multiple_of(source * cap, cap), cap), :] = value

    for t in range(pairs + 5):
        for stage, lag in ((spread, 0), (relay, 1), (finish, 4), (fold, 3), (compute, 2)):
            p = t - lag
            if 0 <= p < pairs:
                if stage is compute and p == 0:
                    for copy in weight_copies:
                        copy.wait()
                stage(p)

    for k in range(1, sp_count):
        expert = flipped(here, k)
        give_back(here, expert).wait_recv()
    mix = chosen[:, 0:1] * jnp.dot(picks[0], returned[...], preferred_element_type=jnp.float32)
    mix = mix + chosen[:, 1:2] * jnp.dot(
        picks[1], returned[...], preferred_element_type=jnp.float32
    )
    out_ref[...] = norm_rows(
        normed_ref[...].astype(jnp.float32) + mix, gains_ref[1:2, :], shifts_ref[1:2, :]
    ).astype(jnp.bfloat16)

    def drain(source, carry):
        to_across(source, me).wait_send()
        to_partner(source, 0, me).wait_send()
        to_partner(source, 1, across).wait_send()
        part_to_partner(source, 0).wait_send()
        part_to_partner(source, 1).wait_send()
        pair_to_across(source).wait_send()

        @pl.when(source != here)
        def _():
            dispatch(source, here).wait_send()
            give_back(source, here).wait_send()
        return carry

    lax.fori_loop(0, sp_count, drain, 0)


def experts(sp_count, tp_count, cap, normed, routes, chosen, gains, shifts, gate, up, down):
    tokens, width = normed.shape
    units = gate.shape[2]
    slots = sp_count * cap
    bf16 = jnp.bfloat16
    dma = pltpu.SemaphoreType.DMA
    any_space = pl.BlockSpec(memory_space=pltpu.HBM)
    return pl.pallas_call(
        functools.partial(experts_kernel, sp_count, tp_count, cap),
        out_shape=jax.ShapeDtypeStruct((tokens, width), bf16),
        in_specs=[VMEM] * 5 + [any_space] * 3,
        out_specs=VMEM,
        scratch_shapes=[
            pltpu.VMEM((slots, width), bf16),
            pltpu.VMEM((slots * tp_count, width), bf16),
            pltpu.VMEM((slots * tp_count, width), bf16),
            pltpu.VMEM((units // 128, width, 256), bf16),
            pltpu.VMEM((units, width), bf16),
            pltpu.VMEM((2 * tp_count * cap, units), bf16),
            pltpu.VMEM((slots * 2, width), bf16),
            pltpu.VMEM((slots, width), bf16),
            pltpu.VMEM((slots, width), bf16),
            pltpu.VMEM((slots, width), bf16),
            pltpu.VMEM((slots, width), bf16),
            dma((2 * (units // 128) + 1,)),
            dma((sp_count,)),
            dma((sp_count,)),
            dma((sp_count,)),
            dma((sp_count,)),
            dma((sp_count, 2)),
            dma((sp_count, 2)),
            dma((sp_count, 2)),
            dma((sp_count, 2)),
            dma((sp_count,)),
            dma((sp_count,)),
            dma((sp_count,)),
            dma((sp_count,)),
        ],
        compiler_params=pltpu.CompilerParams(
            collective_id=1, has_side_effects=True, vmem_limit_bytes=56 * 1024 * 1024
        ),
        name="experts",
    )(normed, routes, chosen, gains, shifts, gate, up, down)


def slot_index(route_rows, block_rows, capacity, expert_count):
    row_total, top_count = route_rows.shape
    sources = row_total // block_rows
    flat_routes = route_rows.reshape(sources, block_rows * top_count)
    expert_marks = (
        flat_routes[:, :, None] == lax.broadcasted_iota(jnp.int32, (1, 1, expert_count), 2)
    ).astype(jnp.int32)
    before = jnp.cumsum(expert_marks, axis=1) - expert_marks
    position = jnp.sum(before * expert_marks, axis=2)
    source_id = lax.broadcasted_iota(jnp.int32, position.shape, 0)
    slots = flat_routes * (sources * capacity) + source_id * capacity + position
    return slots.reshape(row_total, top_count)


def fill_slots(row_block, slots, slot_total):
    owners = lax.broadcasted_iota(jnp.int32, slots.shape, 0).reshape(-1)
    slot_owner = (
        jnp.full((slot_total,), slots.shape[0], jnp.int32).at[slots.reshape(-1)].set(owners)
    )
    return jnp.take(row_block, slot_owner, axis=0, mode="fill", fill_value=0)


def expert_quarter(row_block, gate_part, up_part, down_part):
    gate_val = jnp.dot(row_block, gate_part, preferred_element_type=jnp.float32)
    up_val = jnp.dot(row_block, up_part, preferred_element_type=jnp.float32)
    hidden = (jax.nn.silu(gate_val) * up_val).astype(jnp.bfloat16)
    return jnp.dot(hidden, down_part, preferred_element_type=jnp.float32).astype(jnp.bfloat16)


def combine_rows(returned, slots, weight_rows):
    model_width = returned.shape[-1]
    picked = jnp.take(returned.reshape(-1, model_width), slots.reshape(-1), axis=0)
    picked = picked.reshape(slots.shape + (model_width,))
    return jnp.sum(picked * weight_rows[:, :, None], axis=1)


def on_device(
    residual,
    queries,
    projected_keys,
    values,
    projected_output_gate,
    decay_gate_input,
    decay_gate_offset,
    decay_spikes,
    documents,
    attention_output_weight,
    layer_norm_gains,
    layer_norm_shifts,
    routes,
    chosen_expert_weights,
    expert_gate_weight,
    expert_up_weight,
    expert_down_weight,
):
    sequence_length, head_number = decay_spikes.shape
    rows_dev, model_width = residual.shape
    expert_count = lax.axis_size("sp")
    capacity = max(2, 4 * rows_dev // expert_count)
    normed = attention(
        lax.axis_size("sp"), lax.axis_size("tp"), residual, queries, projected_keys, values,
        projected_output_gate, decay_gate_input, decay_gate_offset, decay_spikes, documents,
        attention_output_weight, layer_norm_gains, layer_norm_shifts,
    )
    peers, parts = lax.axis_size("sp"), lax.axis_size("tp")
    if capacity % 16 == 0 and peers & (peers - 1) == 0 and parts == 4:
        return experts(
            peers, parts, capacity, normed, routes, chosen_expert_weights, layer_norm_gains,
            layer_norm_shifts, expert_gate_weight, expert_up_weight, expert_down_weight,
        )
    own_routes = lax.dynamic_slice_in_dim(routes, lax.axis_index("tp") * rows_dev, rows_dev, 0)
    own_weights = lax.dynamic_slice_in_dim(
        chosen_expert_weights, lax.axis_index("tp") * rows_dev, rows_dev, 0
    )
    slots = slot_index(own_routes, rows_dev, capacity, expert_count)
    outgoing = fill_slots(normed, slots, expert_count * capacity).reshape(
        expert_count, capacity, model_width
    )
    all_rows = lax.all_gather(
        lax.all_to_all(outgoing, "sp", split_axis=0, concat_axis=0, tiled=True),
        "tp",
        axis=1,
        tiled=True,
    )
    sources, slot_count, _ = all_rows.shape
    partial_value = expert_quarter(
        all_rows.reshape(sources * slot_count, model_width),
        expert_gate_weight[0],
        expert_up_weight[0],
        expert_down_weight[0],
    )
    summed = lax.psum_scatter(
        partial_value.reshape(sources, slot_count, model_width)
        .astype(jnp.float32)
        .astype(jnp.bfloat16),
        "tp",
        scatter_dimension=1,
        tiled=True,
    ).astype(jnp.float32)
    returned = lax.all_to_all(
        summed.astype(jnp.bfloat16), "sp", split_axis=0, concat_axis=0, tiled=True
    ).astype(summed.dtype)
    expert_mix = combine_rows(returned, slots, own_weights)
    return norm_rows(
        normed.astype(jnp.float32) + expert_mix, layer_norm_gains[1], layer_norm_shifts[1]
    ).astype(jnp.bfloat16)


def solution(mesh):
    placed = (
        P(("sp", "tp"), None),
        P("sp", "tp"),
        P("sp", "tp"),
        P("sp", "tp"),
        P("sp", "tp"),
        P("sp", "tp"),
        P("tp"),
        P("sp", "tp"),
        P("sp"),
        P("tp", None),
        P(),
        P(),
        P("sp", None),
        P("sp", None),
        P("sp", None, "tp"),
        P("sp", None, "tp"),
        P("sp", "tp", None),
    )
    return jax.shard_map(
        on_device, mesh=mesh, in_specs=placed, out_specs=P(("sp", "tp"), None), check_vma=False
    )
```

profile of v0, /device:TPU:8, one launch (start us, length us, event | category | flops | bytes accessed | tf_op | source)
XLA Modules:
  0.0 111.6 jit_solution(3085051019044342056)
XLA Ops:
  0.0 0.8 copy.21.spikes_ref
  0.8 1.5 %copy.23.routes_ref = s32[256,2]{1,0:T(8,128)} copy(s32[256,2]{0,1:T(2,128)} %param.29) | data formatting | bytes 4096 | tf_op args[12]
  2.3 1.5 %copy.24.chosen_ref = f32[256,2]{1,0:T(8,128)} copy(f32[256,2]{0,1:T(2,128)} %param.30) | data formatting | bytes 4096 | tf_op args[13]
  3.8 0.8 copy.22.doc_col_ref
  4.6 0.0 copy-start.1
  4.6 1.2 %copy-done.1 = bf16[256,2048]{1,0:T(8,128)(2,1)S(1)} copy-done((bf16[256,2048]{1,0:T(8,128)(2,1)S(1)}, bf16[256,2048]{1,0:T(8,128)(2,1)}, u32[]{:S(2)}) %copy-start.1) | copy-done | bytes 1048600
  5.8 0.0 copy-start.2
  5.8 0.9 copy-done.2
  6.7 0.0 copy-start.3
  6.8 0.9 copy-done.3
  7.7 0.0 copy-start.4
  7.7 0.9 copy-done.4
  8.6 0.7 copy-done.5
  9.3 0.7 copy-done.6
  10.0 0.8 copy-done.7
  10.8 0.8 copy-done.8
  11.7 0.8 copy-done.9
  12.5 0.7 copy-done.10
  13.2 0.7 copy-done.11
  13.8 18.7 %attention.1.normed_ref = bf16[64,2048]{1,0:T(8,128)(2,1)S(1)} custom-call(bf16[256,128]{1,0:T(8,128)(2,1)S(1)} %copy-done.7, bf16[256,128]{1,0:T(8,128)(2,1)S(1)} %copy-done.8, bf16[256,256]{1,0:T(8,128)(2,1)S(1)} %copy-done.3, bf16[256,256]{1,0:T(8,128)(2,1)S(1)} %copy-done.4, bf16[256,128]{1,0:T(8,128)(2,1)S(1)} %copy-done.9, f32[1,128]{1,0:T(1,128)S(1)} %bitcast.5, ...), custom_call_target="tpu_custom_call" | custom-call | tf_op jit(solution)/shard_map/attention/pallas_call | solution.py:259
  32.6 0.0 copy-start
  32.6 0.7 copy-done
  33.3 76.6 %experts.1 = bf16[64,2048]{1,0:T(8,128)(2,1)} custom-call(bf16[64,2048]{1,0:T(8,128)(2,1)} %copy-done, s32[256,2]{1,0:T(8,128)} %copy.23.routes_ref, f32[256,2]{1,0:T(8,128)} %copy.24.chosen_ref, f32[2,2048]{1,0:T(2,128)} %gains_ref.3, f32[2,2048]{1,0:T(2,128)} %shifts_ref.3, bf16[1,2048,896]{2,1,0:T(8,128)(2,1)} %gate_hbm.1, bf16[1,2048,896]{2,1,0:T(8,128)(2,1)} %up_hbm.1, ...), custom_call_target="tpu_custom_call" | custom-call | tf_op jit(solution)/shard_map/experts/pallas_call | solution.py:542
  109.9 1.7 %copy.26 = bf16[64,2048]{1,0:T(8,128)(2,1)} copy(bf16[64,2048]{1,0:T(8,128)(2,1)} %experts.1) | data formatting | bytes 524288
  (7 shorter events, 0.0 us)
Async XLA Ops:
  4.6 1.2 %copy-start.1 = (bf16[256,2048]{1,0:T(8,128)(2,1)S(1)}, bf16[256,2048]{1,0:T(8,128)(2,1)}, u32[]{:S(2)}) copy-start(bf16[256,2048]{1,0:T(8,128)(2,1)} %weight_ref.1) | copy-start | bytes 3145732
  5.8 0.9 copy-start.2
  6.7 0.9 copy-start.3
  7.7 0.9 copy-start.4
  8.6 0.7 copy-start.5
  9.3 0.7 copy-start.6
  10.0 0.8 copy-start.7
  10.8 0.8 copy-start.8
  11.7 0.8 copy-start.9
  12.5 0.7 copy-start.10
  13.2 0.7 copy-start.11
  32.6 0.7 copy-start
where the time goes:
time: 112 us
  Pallas kernels  95.3 us (85%)
  local copies, waits for them, and re-layouts  16.2 us (14%)
    pallas_call x1, Pallas kernels, experts(): pl.pallas_call(functools.partial(experts_kernel, sp_count, tp_count, cap)...  76.6 us
    pallas_call x1, Pallas kernels, attention(): pl.pallas_call(functools.partial(attention_kernel, heads, sp_count, tp_co...  18.7 us
    unnamed x28, local copies, waits for them, and re-layouts  15.4 us

commit v1 on v0

--- a/solution.py
+++ b/solution.py
@@ -296,11 +296,39 @@
     return result
 
 
-def experts_kernel(
-    sp_count, tp_count, cap,
-    normed_ref, routes_ref, chosen_ref, gains_ref, shifts_ref, gate_hbm, up_hbm, down_hbm,
+def flipped(index, mask):
+    bit, result = 1, index
+    while bit <= mask:
+        if mask & bit:
+            result = result + bit * (1 - 2 * ((index // bit) % 2))
+        bit *= 2
+    return result
+
+
+END_ORDER = (
+    "S00", "S01", "R00", "S10", "S11", "R01", "C0", "F00", "F01", "R10", "R11", "C1", "S20",
+    "S21", "E00", "E01", "S30", "S31", "F10", "R20", "R21", "C2", "F20", "F21", "R30", "R31",
+    "C3", "F30", "F31", "F11", "E10", "E20", "E21", "E30", "E31", "E11",
+)
+INNER_ORDER = (
+    "S00", "S01", "R00", "S10", "S11", "S20", "S21", "R01", "C0", "R10", "R11", "C1", "S30",
+    "S31", "R20", "R21", "C2", "F20", "F21", "R30", "R31", "C3", "F30", "F31", "F10", "F11",
+    "F00", "F01", "E20", "E21", "E30", "E31", "E10", "E11", "E00", "E01",
+)
+
+
+def layer_kernel(
+    heads, sp_count, tp_count, cap,
+    residual_hbm, q_hbm, k_hbm, v_hbm, gate_hbm, decay_hbm, offset_hbm, spikes_hbm, doc_hbm,
+    routes_hbm, chosen_hbm, weight_hbm, gains_hbm, shifts_hbm, w_gate_hbm, w_up_hbm, w_down_hbm,
     out_ref,
-    outgoing, rows, partial, gate_up, down, hidden, pair_in, far_out, far_in, final, returned,
+    residual_ref, q_ref, k_ref, v_ref, gate_ref, decay_ref, offset_ref, spikes_ref, doc_ref,
+    routes_ref, chosen_ref, weight_ref, gains_ref, shifts_ref,
+    state_out, state_in, state_acc, decay_acc, doc_acc, mixed_ref,
+    part_send, part_in, pair_send, pair_acc,
+    meta_ref, normed_ref,
+    outgoing, rows_ref, partial, gate_up, down, hidden, pair_in, far_out, far_in, final, returned,
+    load_sems, state_send_sem, state_recv_sem, part_send_sem, part_recv_sem, pair_sems,
     weight_sems, a_send, a_recv, y_send, y_recv, p_send, p_recv,
     r_send, r_recv, f_send, f_recv, b_send, b_recv,
 ):
@@ -311,12 +339,30 @@
     partner = side * 2 + (1 - core)
     across = (1 - side) * 2 + core
     diagonal = (1 - side) * 2 + (1 - core)
-    tokens, width = normed_ref.shape
+    rows = q_ref.shape[0]
+    lanes = q_ref.shape[1]
+    key_dim = lanes // heads
+    value_dim = v_ref.shape[1] // heads
+    tokens, width = residual_ref.shape
     slot_total = sp_count * cap
     tile = 128
-    tiles = gate_hbm.shape[2] // tile
+    tiles = w_gate_hbm.shape[2] // tile
     group = 2 * tp_count * cap
-    pairs = sp_count // 2
+
+    loads = [
+        pltpu.make_async_copy(source, target, load_sems.at[n])
+        for n, (source, target) in enumerate(
+            (
+                (decay_hbm, decay_ref), (offset_hbm, offset_ref), (spikes_hbm, spikes_ref),
+                (doc_hbm, doc_ref), (q_hbm, q_ref), (k_hbm, k_ref), (v_hbm, v_ref),
+                (routes_hbm, routes_ref), (chosen_hbm, chosen_ref), (gate_hbm, gate_ref),
+                (weight_hbm, weight_ref), (residual_hbm, residual_ref), (gains_hbm, gains_ref),
+                (shifts_hbm, shifts_ref),
+            )
+        )
+    ]
+    for copy in loads:
+        copy.start()
 
     barrier = pltpu.get_barrier_semaphore()
 
@@ -330,9 +376,12 @@
     pl.semaphore_signal(barrier, inc=1, device_id={"tp": partner}, device_id_type=MESH)
     pl.semaphore_signal(barrier, inc=1, device_id={"tp": across}, device_id_type=MESH)
 
+    for copy in loads[:9]:
+        copy.wait()
+
     weight_copies = []
     for j in range(tiles):
-        for kind, source in enumerate((gate_hbm, up_hbm)):
+        for kind, source in enumerate((w_gate_hbm, w_up_hbm)):
             weight_copies.append(
                 pltpu.make_async_copy(
                     source.at[0, :, pl.ds(j * tile, tile)],
@@ -340,15 +389,188 @@
                     weight_sems.at[2 * j + kind],
                 )
             )
-    weight_copies.append(pltpu.make_async_copy(down_hbm.at[0], down, weight_sems.at[2 * tiles]))
+    weight_copies.append(pltpu.make_async_copy(w_down_hbm.at[0], down, weight_sems.at[2 * tiles]))
     for copy in weight_copies:
         copy.start()
 
+    x = decay_ref[...].astype(jnp.float32) + offset_ref[...]
+    rate = (jnp.minimum(x, 0.0) - jnp.log1p(jnp.exp(-jnp.abs(x)))) * (1.0 / 16.0)
+    extra = jnp.concatenate(
+        [jnp.broadcast_to(spikes_ref[h : h + 1, :], (key_dim, rows)) for h in range(heads)], axis=0
+    ).T
+    doc_row = doc_ref[...].astype(jnp.float32)
+    meta_rows = [routes_ref[j : j + 1, :].astype(jnp.float32) for j in range(2)]
+    meta_rows += [chosen_ref[j : j + 1, :] for j in range(2)]
+    meta = jnp.concatenate(
+        [jnp.broadcast_to(row, (16, rows)) for row in meta_rows]
+        + [jnp.broadcast_to(doc_row, (lanes - 64, rows))],
+        axis=0,
+    ).T
+    meta_ref[...] = meta
+    doc_col = meta[:, 64:65]
+    totals = rate + extra
+    row_of = lax.broadcasted_iota(jnp.int32, rate.shape, 0)
+    step = 1
+    while step < rows:
+        totals = totals + jnp.where(row_of >= step, pltpu.roll(totals, step, 0), 0.0)
+        step *= 2
+    last_total = totals[rows - 1 : rows, :]
+    last_doc = doc_row[:, rows - 1 : rows]
+    key = k_ref[...].astype(jnp.float32)
+    query = q_ref[...].astype(jnp.float32) * key_dim ** (-0.5)
+    ends = (key * jnp.exp(last_total - totals) * (doc_col == last_doc).astype(jnp.float32)).astype(
+        jnp.bfloat16
+    )
+    values = v_ref[...]
+    state = jnp.concatenate(
+        [
+            lax.dot_general(
+                values[:, h * value_dim : (h + 1) * value_dim],
+                ends[:, h * key_dim : (h + 1) * key_dim],
+                TN,
+                preferred_element_type=jnp.float32,
+            )
+            for h in range(heads)
+        ],
+        axis=1,
+    )
+    state_out[0:value_dim, :] = state.astype(jnp.bfloat16)
+    tail_shape = (state_out.shape[0] - value_dim, lanes)
+    tail_row = lax.broadcasted_iota(jnp.int32, tail_shape, 0)
+    state_out[value_dim:, :] = jnp.where(
+        tail_row == 0, jnp.exp(last_total), jnp.broadcast_to(last_doc, tail_shape)
+    ).astype(jnp.bfloat16)
+    pl.semaphore_wait(barrier, sp_count + 1)
+
+    def state_copy(target, slot):
+        return pltpu.make_async_remote_copy(
+            src_ref=state_out,
+            dst_ref=state_in.at[slot],
+            send_sem=state_send_sem.at[target],
+            recv_sem=state_recv_sem.at[slot],
+            device_id={"sp": target},
+            device_id_type=MESH,
+        )
+
+    def send_state(j, carry):
+        target = sp_count - 1 - j
+
+        @pl.when(target > here)
+        def _():
+            state_copy(target, here).start()
+        return carry
+
+    lax.fori_loop(0, sp_count, send_state, 0)
+
+    t_of = lax.broadcasted_iota(jnp.int32, (rows, rows), 0)
+    s_of = lax.broadcasted_iota(jnp.int32, (rows, rows), 1)
+    apart = t_of ^ s_of
+    visible = (t_of >= s_of) & (doc_col == doc_row)
+    halves = []
+    half = 1
+    while half < rows:
+        halves.append(half)
+        half *= 2
+    scaled = [(0, query.astype(jnp.bfloat16), k_ref[...])]
+    for half in halves:
+        fade = jnp.exp(-jnp.abs(totals - halfway_totals(totals, half)))
+        scaled.append((half, (query * fade).astype(jnp.bfloat16), (key * fade).astype(jnp.bfloat16)))
+    inner = []
+    for h in range(heads):
+        span = slice(h * key_dim, (h + 1) * key_dim)
+        scores = None
+        for half, q_part, k_part in scaled:
+            product = lax.dot_general(
+                q_part[:, span], k_part[:, span], NT, preferred_element_type=jnp.float32
+            )
+            scores = product if scores is None else jnp.where(apart >= half, product, scores)
+        scores = jnp.where(visible, scores, 0.0).astype(jnp.bfloat16)
+        inner.append(
+            jnp.dot(
+                scores,
+                values[:, h * value_dim : (h + 1) * value_dim],
+                preferred_element_type=jnp.float32,
+            )
+        )
+
+    state_acc[...] = jnp.zeros_like(state_acc)
+    decay_acc[...] = jnp.ones_like(decay_acc)
+    doc_acc[...] = jnp.full_like(doc_acc, -1.0)
+
+    def join(j, carry):
+        k = here - 1 - j
+
+        @pl.when(k >= 0)
+        def _():
+            state_copy(here, k).wait_recv()
+            tail = state_in[k, value_dim:, :].astype(jnp.float32)
+            doc_k = tail[1:2, :]
+
+            @pl.when(j == 0)
+            def _():
+                doc_acc[...] = doc_k
+
+            factor = jnp.where(doc_k == doc_acc[...], decay_acc[...], 0.0)
+            state_acc[...] += state_in[k, 0:value_dim, :].astype(jnp.float32) * factor
+            decay_acc[...] = factor * tail[0:1, :]
+        return carry
+
+    lax.fori_loop(0, sp_count, join, 0)
+    for copy in loads[9:]:
+        copy.wait()
+    prefix = state_acc[...].astype(jnp.bfloat16)
+    active = (doc_col == doc_acc[...]).astype(jnp.float32)
+    entering = (query * jnp.exp(totals) * active).astype(jnp.bfloat16)
+    for h in range(heads):
+        span = slice(h * key_dim, (h + 1) * key_dim)
+        out_span = slice(h * value_dim, (h + 1) * value_dim)
+        recurrent = inner[h] + lax.dot_general(
+            entering[:, span], prefix[:, span], NT, preferred_element_type=jnp.float32
+        )
+        scale = lax.rsqrt(jnp.mean(recurrent * recurrent, axis=-1, keepdims=True) + 1e-6)
+        gate = silu(gate_ref[:, out_span].astype(jnp.float32))
+        mixed_ref[:, out_span] = (recurrent * scale * gate).astype(jnp.bfloat16)
+
+    def share(index):
+        begin = pl.multiple_of(index * tokens, tokens)
+        return jnp.dot(
+            mixed_ref[pl.ds(begin, tokens), :], weight_ref[...], preferred_element_type=jnp.float32
+        )
+
+    def part_copy(slot):
+        return pltpu.make_async_remote_copy(
+            src_ref=part_send.at[slot],
+            dst_ref=part_in.at[slot],
+            send_sem=part_send_sem.at[slot],
+            recv_sem=part_recv_sem.at[slot],
+            device_id={"tp": partner},
+            device_id_type=MESH,
+        )
+
+    pair_copy = pltpu.make_async_remote_copy(
+        src_ref=pair_send,
+        dst_ref=pair_acc,
+        send_sem=pair_sems.at[0],
+        recv_sem=pair_sems.at[1],
+        device_id={"tp": across},
+        device_id_type=MESH,
+    )
+    part_send[0] = share(diagonal).astype(jnp.bfloat16)
+    part_copy(0).start()
+    far = share(across)
+    part_copy(0).wait_recv()
+    pair_send[...] = (far + part_in[0].astype(jnp.float32)).astype(jnp.bfloat16)
+    pair_copy.start()
+    part_send[1] = share(partner).astype(jnp.bfloat16)
+    part_copy(1).start()
+    near = share(me) + residual_ref[...].astype(jnp.float32)
+
     begin = pl.multiple_of(me * tokens, tokens)
-    routes = routes_ref[pl.ds(begin, tokens), :]
-    chosen = chosen_ref[pl.ds(begin, tokens), :]
-    expert_lane = lax.broadcasted_iota(jnp.int32, (tokens, 128), 1)
-    marks = [(routes[:, j : j + 1] == expert_lane).astype(jnp.float32) for j in range(2)]
+    own_meta = meta_ref[pl.ds(begin, tokens), :]
+    routes = [own_meta[:, 16 * j : 16 * j + 1] for j in range(2)]
+    chosen = [own_meta[:, 32 + 16 * j : 33 + 16 * j] for j in range(2)]
+    expert_lane = lax.broadcasted_iota(jnp.int32, (tokens, 128), 1).astype(jnp.float32)
+    marks = [(routes[j] == expert_lane).astype(jnp.float32) for j in range(2)]
     earlier = (
         lax.broadcasted_iota(jnp.int32, (tokens, tokens), 0)
         > lax.broadcasted_iota(jnp.int32, (tokens, tokens), 1)
@@ -362,8 +584,14 @@
     picks = []
     for j in range(2):
         position = jnp.sum(before * marks[j], axis=1, keepdims=True)
-        slot = routes[:, j : j + 1].astype(jnp.float32) * float(cap) + position
+        slot = routes[j] * float(cap) + position
         picks.append((slot_lane == slot).astype(jnp.bfloat16))
+
+    part_copy(1).wait_recv()
+    near = near + part_in[1].astype(jnp.float32)
+    pair_copy.wait_recv()
+    near = near + pair_acc[...].astype(jnp.float32)
+    normed_ref[...] = norm_rows(near, gains_ref[0:1, :], shifts_ref[0:1, :]).astype(jnp.bfloat16)
     outgoing[...] = lax.dot_general(
         picks[0] + picks[1], normed_ref[...], TN, preferred_element_type=jnp.float32
     ).astype(jnp.bfloat16)
@@ -381,7 +609,7 @@
         )
 
     def row_block(source, part):
-        return block(rows, source * tp_count + part)
+        return block(rows_ref, source * tp_count + part)
 
     def dispatch(target, source):
         return remote(
@@ -420,37 +648,45 @@
             {"sp": source},
         )
 
-    pl.semaphore_wait(barrier, sp_count + 1)
-    for k in range(1, sp_count):
-        dispatch(flipped(here, k), here).start()
+    chain = here // 2
+    upper = chain // 2
+    levels = (chain, flipped(chain, 1), 2 - upper, 3 - 3 * upper)
+
+    def sources_of(i):
+        base = levels[i] * 2
+        return (base + here % 2, base + 1 - here % 2)
+
     own = pl.multiple_of((here * tp_count + me) * cap, cap)
-    rows[pl.ds(own, cap), :] = load(outgoing, here)
-
-    def sources_of(p):
-        base = flipped(here // 2, p) * 2
-        return (base + here % 2, base + 1 - here % 2)
-
-    def spread(p):
-        for n, source in enumerate(sources_of(p)):
-            if p or n:
-                dispatch(source, source).wait_recv()
-            to_across(source, me).start()
-            to_partner(source, 0, me).start()
-
-    def relay(p):
-        for source in sources_of(p):
-            to_across(source, across).wait_recv()
-            to_partner(source, 1, across).start()
-
-    def compute(p):
-        for source in sources_of(p):
+    rows_ref[pl.ds(own, cap), :] = load(outgoing, here)
+    for i in range(4):
+        for n, target in enumerate(sources_of(i)):
+            if i or n:
+                dispatch(target, here).start()
+
+    def spread(i, n):
+        source = sources_of(i)[n]
+        if i or n:
+            dispatch(source, source).wait_recv()
+        to_across(source, me).start()
+        to_partner(source, 0, me).start()
+
+    def relay(i, n):
+        source = sources_of(i)[n]
+        to_across(source, across).wait_recv()
+        to_partner(source, 1, across).start()
+
+    def compute(i):
+        for source in sources_of(i):
             to_partner(source, 0, partner).wait_recv()
             to_partner(source, 1, diagonal).wait_recv()
-        base = pl.multiple_of(flipped(here // 2, p) * group, group)
+        if i == 0:
+            for copy in weight_copies:
+                copy.wait()
+        base = pl.multiple_of(levels[i] * group, group)
 
         def first(j, carry):
             both = jnp.dot(
-                rows[pl.ds(base, group), :], gate_up[j], preferred_element_type=jnp.float32
+                rows_ref[pl.ds(base, group), :], gate_up[j], preferred_element_type=jnp.float32
             )
             unit = (silu(both[:, :tile]) * both[:, tile:]).astype(jnp.bfloat16)
             hidden[:, pl.ds(pl.multiple_of(j * tile, tile), tile)] = unit
@@ -460,62 +696,74 @@
         span = 512
 
         def second(j, carry):
-            lanes = pl.ds(pl.multiple_of(j * span, span), span)
-            partial[pl.ds(base, group), lanes] = jnp.dot(
-                hidden[...], down[:, lanes], preferred_element_type=jnp.float32
+            columns = pl.ds(pl.multiple_of(j * span, span), span)
+            partial[pl.ds(base, group), columns] = jnp.dot(
+                hidden[...], down[:, columns], preferred_element_type=jnp.float32
             ).astype(jnp.bfloat16)
             return carry
 
         lax.fori_loop(0, width // span, second, 0)
         for turn in (1, 0):
-            for source in sources_of(p):
+            for source in sources_of(i):
                 part_to_partner(source, turn).start()
 
-    def fold(p):
-        for source in sources_of(p):
-            part_to_partner(source, 1).wait_recv()
-            far_out[pl.ds(pl.multiple_of(source * cap, cap), cap), :] = (
-                load(partial, source * tp_count + across).astype(jnp.float32)
-                + load(pair_in, source * 2 + 1).astype(jnp.float32)
-            ).astype(jnp.bfloat16)
-            pair_to_across(source).start()
-
-    def finish(p):
-        for n, source in enumerate(sources_of(p)):
-            part_to_partner(source, 0).wait_recv()
-            pair_to_across(source).wait_recv()
-            value = (
-                load(partial, source * tp_count + me).astype(jnp.float32)
-                + load(pair_in, source * 2).astype(jnp.float32)
-                + load(far_in, source).astype(jnp.float32)
-            ).astype(jnp.bfloat16)
-            if p or n:
-                final[pl.ds(pl.multiple_of(source * cap, cap), cap), :] = value
-                give_back(source, here).start()
-            else:
-                returned[pl.ds(pl.multiple_of(source * cap, cap), cap), :] = value
-
-    for t in range(pairs + 5):
-        for stage, lag in ((spread, 0), (relay, 1), (finish, 4), (fold, 3), (compute, 2)):
-            p = t - lag
-            if 0 <= p < pairs:
-                if stage is compute and p == 0:
-                    for copy in weight_copies:
-                        copy.wait()
-                stage(p)
-
-    for k in range(1, sp_count):
-        expert = flipped(here, k)
-        give_back(here, expert).wait_recv()
-    mix = chosen[:, 0:1] * jnp.dot(picks[0], returned[...], preferred_element_type=jnp.float32)
-    mix = mix + chosen[:, 1:2] * jnp.dot(
-        picks[1], returned[...], preferred_element_type=jnp.float32
-    )
+    def fold(i, n):
+        source = sources_of(i)[n]
+        part_to_partner(source, 1).wait_recv()
+        far_out[pl.ds(pl.multiple_of(source * cap, cap), cap), :] = (
+            load(partial, source * tp_count + across).astype(jnp.float32)
+            + load(pair_in, source * 2 + 1).astype(jnp.float32)
+        ).astype(jnp.bfloat16)
+        pair_to_across(source).start()
+
+    def finish(i, n):
+        source = sources_of(i)[n]
+        part_to_partner(source, 0).wait_recv()
+        pair_to_across(source).wait_recv()
+        value = (
+            load(partial, source * tp_count + me).astype(jnp.float32)
+            + load(pair_in, source * 2).astype(jnp.float32)
+            + load(far_in, source).astype(jnp.float32)
+        ).astype(jnp.bfloat16)
+        if i or n:
+            final[pl.ds(pl.multiple_of(source * cap, cap), cap), :] = value
+            give_back(source, here).start()
+        else:
+            returned[pl.ds(pl.multiple_of(source * cap, cap), cap), :] = value
+
+    stages = {"S": spread, "R": relay, "F": fold, "E": finish, "C": compute}
+
+    def run(order):
+        for item in order:
+            stages[item[0]](*[int(digit) for digit in item[1:]])
+
+    @pl.when(chain % 3 == 0)
+    def _():
+        run(END_ORDER)
+
+    @pl.when(chain % 3 != 0)
+    def _():
+        run(INNER_ORDER)
+
+    for i in range(4):
+        for n, expert in enumerate(sources_of(i)):
+            if i or n:
+                give_back(here, expert).wait_recv()
+    mix = chosen[0] * jnp.dot(picks[0], returned[...], preferred_element_type=jnp.float32)
+    mix = mix + chosen[1] * jnp.dot(picks[1], returned[...], preferred_element_type=jnp.float32)
     out_ref[...] = norm_rows(
         normed_ref[...].astype(jnp.float32) + mix, gains_ref[1:2, :], shifts_ref[1:2, :]
     ).astype(jnp.bfloat16)
 
+    part_copy(0).wait_send()
+    part_copy(1).wait_send()
+    pair_copy.wait_send()
+
     def drain(source, carry):
+        @pl.when(source > here)
+        def _():
+            state_copy(source, here).wait_send()
+
         to_across(source, me).wait_send()
         to_partner(source, 0, me).wait_send()
         to_partner(source, 1, across).wait_send()
@@ -532,19 +780,41 @@
     lax.fori_loop(0, sp_count, drain, 0)
 
 
-def experts(sp_count, tp_count, cap, normed, routes, chosen, gains, shifts, gate, up, down):
-    tokens, width = normed.shape
-    units = gate.shape[2]
+def layer(
+    sp_count, tp_count, cap, residual, q, k, v, gate, decay_in, offset, spikes, documents, weight,
+    gains, shifts, routes, chosen, w_gate, w_up, w_down,
+):
+    rows, heads = spikes.shape
+    tokens, width = residual.shape
+    channels = q.shape[1]
+    units = w_gate.shape[2]
     slots = sp_count * cap
-    bf16 = jnp.bfloat16
+    state_rows = v.shape[1] // heads + 16
+    bf16, f32 = jnp.bfloat16, jnp.float32
     dma = pltpu.SemaphoreType.DMA
-    any_space = pl.BlockSpec(memory_space=pltpu.HBM)
+    inputs = (
+        residual, q, k, v, gate, decay_in, offset.reshape(1, -1), spikes.T,
+        documents.reshape(1, -1), routes.T, chosen.T, weight, gains, shifts, w_gate, w_up, w_down,
+    )
     return pl.pallas_call(
-        functools.partial(experts_kernel, sp_count, tp_count, cap),
+        functools.partial(layer_kernel, heads, sp_count, tp_count, cap),
         out_shape=jax.ShapeDtypeStruct((tokens, width), bf16),
-        in_specs=[VMEM] * 5 + [any_space] * 3,
+        in_specs=[pl.BlockSpec(memory_space=pltpu.HBM)] * len(inputs),
         out_specs=VMEM,
-        scratch_shapes=[
+        scratch_shapes=[pltpu.VMEM(value.shape, value.dtype) for value in inputs[:14]]
+        + [
+            pltpu.VMEM((state_rows, channels), bf16),
+            pltpu.VMEM((sp_count, state_rows, channels), bf16),
+            pltpu.VMEM((state_rows - 16, channels), f32),
+            pltpu.VMEM((1, channels), f32),
+            pltpu.VMEM((1, channels), f32),
+            pltpu.VMEM((rows, v.shape[1]), bf16),
+            pltpu.VMEM((2, tokens, width), bf16),
+            pltpu.VMEM((2, tokens, width), bf16),
+            pltpu.VMEM((tokens, width), bf16),
+            pltpu.VMEM((tokens, width), bf16),
+            pltpu.VMEM((rows, channels), f32),
+            pltpu.VMEM((tokens, width), bf16),
             pltpu.VMEM((slots, width), bf16),
             pltpu.VMEM((slots * tp_count, width), bf16),
             pltpu.VMEM((slots * tp_count, width), bf16),
@@ -556,6 +826,12 @@
             pltpu.VMEM((slots, width), bf16),
             pltpu.VMEM((slots, width), bf16),
             pltpu.VMEM((slots, width), bf16),
+            dma((14,)),
+            dma((sp_count,)),
+            dma((sp_count,)),
+            dma((2,)),
+            dma((2,)),
+            dma((2,)),
             dma((2 * (units // 128) + 1,)),
             dma((sp_count,)),
             dma((sp_count,)),
@@ -571,10 +847,10 @@
             dma((sp_count,)),
         ],
         compiler_params=pltpu.CompilerParams(
-            collective_id=1, has_side_effects=True, vmem_limit_bytes=56 * 1024 * 1024
+            collective_id=1, has_side_effects=True, vmem_limit_bytes=67043328
         ),
-        name="experts",
-    )(normed, routes, chosen, gains, shifts, gate, up, down)
+        name="layer",
+    )(*inputs)
 
 
 def slot_index(route_rows, block_rows, capacity, expert_count):
@@ -636,17 +912,23 @@
     rows_dev, model_width = residual.shape
     expert_count = lax.axis_size("sp")
     capacity = max(2, 4 * rows_dev // expert_count)
+    peers, parts = lax.axis_size("sp"), lax.axis_size("tp")
+    channels = queries.shape[1]
+    if (
+        capacity % 16 == 0 and peers == 8 and parts == 4 and channels == 128
+        and sequence_length % 128 == 0
+    ):
+        return layer(
+            peers, parts, capacity, residual, queries, projected_keys, values,
+            projected_output_gate, decay_gate_input, decay_gate_offset, decay_spikes, documents,
+            attention_output_weight, layer_norm_gains, layer_norm_shifts, routes,
+            chosen_expert_weights, expert_gate_weight, expert_up_weight, expert_down_weight,
+        )
     normed = attention(
-        lax.axis_size("sp"), lax.axis_size("tp"), residual, queries, projected_keys, values,
+        peers, parts, residual, queries, projected_keys, values,
         projected_output_gate, decay_gate_input, decay_gate_offset, decay_spikes, documents,
         attention_output_weight, layer_norm_gains, layer_norm_shifts,
     )
-    peers, parts = lax.axis_size("sp"), lax.axis_size("tp")
-    if capacity % 16 == 0 and peers & (peers - 1) == 0 and parts == 4:
-        return experts(
-            peers, parts, capacity, normed, routes, chosen_expert_weights, layer_norm_gains,
-            layer_norm_shifts, expert_gate_weight, expert_up_weight, expert_down_weight,
-        )
     own_routes = lax.dynamic_slice_in_dim(routes, lax.axis_index("tp") * rows_dev, rows_dev, 0)
     own_weights = lax.dynamic_slice_in_dim(
         chosen_expert_weights, lax.axis_index("tp") * rows_dev, rows_dev, 0

time: 112 us -> 100 us (0.89)
  the two profiles are of different devices: /device:TPU:8 before, /device:TPU:0 now
where the time goes in v1:
time: 100 us; the launch traced here: 99.9 us
  Pallas kernels  98.3 us (98%)
  local copies, waits for them, and re-layouts  1.67 us (2%)
    pallas_call x1, Pallas kernels, layer(): pl.pallas_call(functools.partial(layer_kernel, heads, sp_count, tp_count,...  98.3 us

profile of v1, /device:TPU:0, one launch (start us, length us, event | category | flops | bytes accessed | tf_op | source)
XLA Modules:
  0.0 99.9 jit_solution(8747711123261251812)
XLA Ops:
  0.0 98.3 %layer.1 = bf16[64,2048]{1,0:T(8,128)(2,1)} custom-call(bf16[64,2048]{1,0:T(8,128)(2,1)} %residual_hbm.1, bf16[256,128]{1,0:T(8,128)(2,1)} %q_hbm.1, bf16[256,128]{1,0:T(8,128)(2,1)} %k_hbm.1, bf16[256,256]{1,0:T(8,128)(2,1)} %v_hbm.1, bf16[256,256]{1,0:T(8,128)(2,1)} %gate_hbm.1, bf16[256,128]{1,0:T(8,128)(2,1)} %decay_hbm.1, f32[1,128]{1,0:T(1,128)} %bitcast.9, ...), custom_call_target="tpu_custom_call" | custom-call | tf_op jit(solution)/shard_map/layer/pallas_call | solution.py:799
  98.3 1.7 %copy.19 = bf16[64,2048]{1,0:T(8,128)(2,1)} copy(bf16[64,2048]{1,0:T(8,128)(2,1)} %layer.1) | data formatting | bytes 524288

commit v2 on v1

--- a/solution.py
+++ b/solution.py
@@ -305,15 +305,28 @@
     return result
 
 
-END_ORDER = (
-    "S00", "S01", "R00", "S10", "S11", "R01", "C0", "F00", "F01", "R10", "R11", "C1", "S20",
-    "S21", "E00", "E01", "S30", "S31", "F10", "R20", "R21", "C2", "F20", "F21", "R30", "R31",
-    "C3", "F30", "F31", "F11", "E10", "E20", "E21", "E30", "E31", "E11",
+END_PLAN = (
+    ("D01", "D20", "D21", "S00", "S01", "R00", "S10", "D10", "D11", "R01", "W0", "D30", "D31",),
+    ("S20",),
+    ("S11", "R10", "S21", "R11", "S30", "W1",),
+    ("S31",),
+    ("F10", "F11", "R20", "R21", "W2",),
+    ("R30",),
+    ("R31", "F01", "W3",),
+    ("E10",),
+    ("F30", "F31", "E11", "F20", "F21", "F00", "E01", "E30", "E31", "E20", "E21", "E00",),
 )
-INNER_ORDER = (
-    "S00", "S01", "R00", "S10", "S11", "S20", "S21", "R01", "C0", "R10", "R11", "C1", "S30",
-    "S31", "R20", "R21", "C2", "F20", "F21", "R30", "R31", "C3", "F30", "F31", "F10", "F11",
-    "F00", "F01", "E20", "E21", "E30", "E31", "E10", "E11", "E00", "E01",
+INNER_PLAN = (
+    ("D01", "D10", "D11", "D20", "D21", "S00", "S10", "S01", "R00", "S11", "S20", "R01", "W0",
+     "D30", "D31",),
+    ("S21",),
+    ("R10", "R11", "F01", "W1",),
+    ("S30",),
+    ("R20", "R21", "S31", "F10", "W2",),
+    (),
+    ("F20", "F21", "R30", "R31", "W3",),
+    ("E01",),
+    ("F30", "F31", "E20", "E21", "F11", "F00", "E10", "E30", "E31", "E11", "E00",),
 )
 
 
@@ -440,6 +453,28 @@
     state_out[value_dim:, :] = jnp.where(
         tail_row == 0, jnp.exp(last_total), jnp.broadcast_to(last_doc, tail_shape)
     ).astype(jnp.bfloat16)
+    begin = pl.multiple_of(me * tokens, tokens)
+    own_meta = meta_ref[pl.ds(begin, tokens), :]
+    routes = [own_meta[:, 16 * j : 16 * j + 1] for j in range(2)]
+    chosen = [own_meta[:, 32 + 16 * j : 33 + 16 * j] for j in range(2)]
+    expert_lane = lax.broadcasted_iota(jnp.int32, (tokens, 128), 1).astype(jnp.float32)
+    marks = [(routes[j] == expert_lane).astype(jnp.float32) for j in range(2)]
+    earlier = (
+        lax.broadcasted_iota(jnp.int32, (tokens, tokens), 0)
+        > lax.broadcasted_iota(jnp.int32, (tokens, tokens), 1)
+    ).astype(jnp.float32)
+    before = jnp.dot(
+        earlier.astype(jnp.bfloat16),
+        (marks[0] + marks[1]).astype(jnp.bfloat16),
+        preferred_element_type=jnp.float32,
+    )
+    slot_lane = lax.broadcasted_iota(jnp.int32, (tokens, slot_total), 1).astype(jnp.float32)
+    picks = []
+    for j in range(2):
+        position = jnp.sum(before * marks[j], axis=1, keepdims=True)
+        slot = routes[j] * float(cap) + position
+        picks.append((slot_lane == slot).astype(jnp.bfloat16))
+
     pl.semaphore_wait(barrier, sp_count + 1)
 
     def state_copy(target, slot):
@@ -565,28 +600,6 @@
     part_copy(1).start()
     near = share(me) + residual_ref[...].astype(jnp.float32)
 
-    begin = pl.multiple_of(me * tokens, tokens)
-    own_meta = meta_ref[pl.ds(begin, tokens), :]
-    routes = [own_meta[:, 16 * j : 16 * j + 1] for j in range(2)]
-    chosen = [own_meta[:, 32 + 16 * j : 33 + 16 * j] for j in range(2)]
-    expert_lane = lax.broadcasted_iota(jnp.int32, (tokens, 128), 1).astype(jnp.float32)
-    marks = [(routes[j] == expert_lane).astype(jnp.float32) for j in range(2)]
-    earlier = (
-        lax.broadcasted_iota(jnp.int32, (tokens, tokens), 0)
-        > lax.broadcasted_iota(jnp.int32, (tokens, tokens), 1)
-    ).astype(jnp.float32)
-    before = jnp.dot(
-        earlier.astype(jnp.bfloat16),
-        (marks[0] + marks[1]).astype(jnp.bfloat16),
-        preferred_element_type=jnp.float32,
-    )
-    slot_lane = lax.broadcasted_iota(jnp.int32, (tokens, slot_total), 1).astype(jnp.float32)
-    picks = []
-    for j in range(2):
-        position = jnp.sum(before * marks[j], axis=1, keepdims=True)
-        slot = routes[j] * float(cap) + position
-        picks.append((slot_lane == slot).astype(jnp.bfloat16))
-
     part_copy(1).wait_recv()
     near = near + part_in[1].astype(jnp.float32)
     pair_copy.wait_recv()
@@ -650,7 +663,15 @@
 
     chain = here // 2
     upper = chain // 2
-    levels = (chain, flipped(chain, 1), 2 - upper, 3 - 3 * upper)
+    near, inner_far, end_far = flipped(chain, 1), 2 - upper, 3 - 3 * upper
+    at_end = chain % 3 == 0
+    ending = at_end.astype(jnp.int32)
+    levels = (
+        chain,
+        near + ending * (inner_far - near),
+        end_far + ending * (near - end_far),
+        inner_far + ending * (end_far - inner_far),
+    )
 
     def sources_of(i):
         base = levels[i] * 2
@@ -658,10 +679,9 @@
 
     own = pl.multiple_of((here * tp_count + me) * cap, cap)
     rows_ref[pl.ds(own, cap), :] = load(outgoing, here)
-    for i in range(4):
-        for n, target in enumerate(sources_of(i)):
-            if i or n:
-                dispatch(target, here).start()
+
+    def send(i, n):
+        dispatch(sources_of(i)[n], here).start()
 
     def spread(i, n):
         source = sources_of(i)[n]
@@ -675,13 +695,12 @@
         to_across(source, across).wait_recv()
         to_partner(source, 1, across).start()
 
-    def compute(i):
+    def gathered(i):
         for source in sources_of(i):
             to_partner(source, 0, partner).wait_recv()
             to_partner(source, 1, diagonal).wait_recv()
-        if i == 0:
-            for copy in weight_copies:
-                copy.wait()
+
+    def compute(i):
         base = pl.multiple_of(levels[i] * group, group)
 
         def first(j, carry):
@@ -692,7 +711,10 @@
             hidden[:, pl.ds(pl.multiple_of(j * tile, tile), tile)] = unit
             return carry
 
-        lax.fori_loop(0, tiles, first, 0)
+        lax.fori_loop(0, tiles, first, 0, unroll=True)
+
+    def project(i):
+        base = pl.multiple_of(levels[i] * group, group)
         span = 512
 
         def second(j, carry):
@@ -702,7 +724,7 @@
             ).astype(jnp.bfloat16)
             return carry
 
-        lax.fori_loop(0, width // span, second, 0)
+        lax.fori_loop(0, width // span, second, 0, unroll=True)
         for turn in (1, 0):
             for source in sources_of(i):
                 part_to_partner(source, turn).start()
@@ -731,19 +753,21 @@
         else:
             returned[pl.ds(pl.multiple_of(source * cap, cap), cap), :] = value
 
-    stages = {"S": spread, "R": relay, "F": fold, "E": finish, "C": compute}
+    stages = {"D": send, "S": spread, "R": relay, "W": gathered, "F": fold, "E": finish}
 
     def run(order):
         for item in order:
             stages[item[0]](*[int(digit) for digit in item[1:]])
 
-    @pl.when(chain % 3 == 0)
-    def _():
-        run(END_ORDER)
-
-    @pl.when(chain % 3 != 0)
-    def _():
-        run(INNER_ORDER)
+    for copy in weight_copies:
+        copy.wait()
+    for i in range(9):
+        if END_PLAN[i]:
+            pl.when(at_end)(functools.partial(run, END_PLAN[i]))
+        if INNER_PLAN[i]:
+            pl.when(jnp.logical_not(at_end))(functools.partial(run, INNER_PLAN[i]))
+        if i < 8:
+            (project if i % 2 else compute)(i // 2)
 
     for i in range(4):
         for n, expert in enumerate(sources_of(i)):

time: 100 us -> 87.7 us (0.88)
  the two profiles are of different devices: /device:TPU:0 before, /device:TPU:11 now
where the time goes in v2:
time: 87.7 us; the launch traced here: 87.5 us
  Pallas kernels  85.9 us (98%)
  local copies, waits for them, and re-layouts  1.67 us (2%)
    pallas_call x1, Pallas kernels, layer(): pl.pallas_call(functools.partial(layer_kernel, heads, sp_count, tp_count,...  85.9 us

profile of v2, /device:TPU:11, one launch (start us, length us, event | category | flops | bytes accessed | tf_op | source)
XLA Modules:
  0.0 87.5 jit_solution(10374667862381208868)
XLA Ops:
  0.0 85.9 %layer.1 = bf16[64,2048]{1,0:T(8,128)(2,1)} custom-call(bf16[64,2048]{1,0:T(8,128)(2,1)} %residual_hbm.1, bf16[256,128]{1,0:T(8,128)(2,1)} %q_hbm.1, bf16[256,128]{1,0:T(8,128)(2,1)} %k_hbm.1, bf16[256,256]{1,0:T(8,128)(2,1)} %v_hbm.1, bf16[256,256]{1,0:T(8,128)(2,1)} %gate_hbm.1, bf16[256,128]{1,0:T(8,128)(2,1)} %decay_hbm.1, f32[1,128]{1,0:T(1,128)} %bitcast.9, ...), custom_call_target="tpu_custom_call" | custom-call | tf_op jit(solution)/shard_map/layer/pallas_call | solution.py:823
  85.9 1.7 %copy.19 = bf16[64,2048]{1,0:T(8,128)(2,1)} copy(bf16[64,2048]{1,0:T(8,128)(2,1)} %layer.1) | data formatting | bytes 524288
